TPU v7x, 512 devices: a whole 4x8x8 slice. The times are simulated.
512 devices in a mesh: row: 32 (over z, x), col: 16 (over y, core).
Axes of the slice: x: 4, y: 8, z: 8, core: 2. Of those that a mesh axis runs over, the one named last changes fastest.
Arguments:
- tokens: bfloat16 [32768, 2048], P('row'), may hold values from -136 to 136
- norm_gain: float32 [2048], replicated, may hold values from 0.1 to 1.9
- w_in: bfloat16 [2048, 1024], P(None, 'col'), may hold values from -0.125 to 0.125
- w_out: bfloat16 [1024, 2048], P(None, 'col'), may hold values from -0.1875 to 0.1875
Outputs:
- mixed_tokens: bfloat16 [32768, 2048], P('row', 'col')
All inputs are finite; a program needn't handle non-finite values.
Results may differ from a plain program's by a relative error of at most 0.013.
Values may be sent and summed in bfloat16 or wider, within the bound.
No kernel may reach another device: no remote copies, remote signals or barrier semaphores. Data moves between devices by JAX's collectives and lax.ppermute only.
A program may use at most 64 MiB of HBM per device.

v0:
```python
import math
import jax
import jax.numpy as jnp
from jax import lax
from jax.sharding import PartitionSpec as P

GROUP = 256
NORM_EPS = 1e-06


def in_one_piece(arrays, axis, split_dim, concat_dim, along):
    ends, at = ([], 0)
    for a in arrays[:-1]:
        at += a.shape[along]
        ends.append(at)
    both = jnp.concatenate(arrays, axis=along)
    return tuple(
        jnp.split(
            lax.all_to_all(both, axis, split_axis=split_dim, concat_axis=concat_dim, tiled=True),
            ends,
            axis=along,
        )
    )


def as_sent(array):

    def short(part):
        return part.astype(jnp.bfloat16) if part.dtype == jnp.float32 else part

    return jax.tree.map(short, array)


def rotation_table(first_index, second_index, spectral_magnitude, factor):
    phase = (first_index * second_index % spectral_magnitude).astype(jnp.float32) * (
        2.0 * math.pi / spectral_magnitude
    )
    return (jnp.cos(phase) * factor, jnp.sin(phase) * factor)


def twiddle(real_input_values, imag_in, freq_index, pos_index, spectral_magnitude):
    cosine, sine = rotation_table(freq_index, pos_index, spectral_magnitude, 1.0)
    return (
        real_input_values * cosine + imag_in * sine,
        imag_in * cosine - real_input_values * sine,
    )


def second_section(stacked, half):
    length_dev = stacked.shape[1]
    stride = min(length_dev, 512)
    positions = lax.broadcasted_iota(jnp.int32, (length_dev, stride), 0)
    real_blocks = []
    imag_blocks = []
    for offset in range(0, length_dev, stride):
        freqs = lax.broadcasted_iota(jnp.int32, (length_dev, stride), 1) + offset
        cosine, sine = rotation_table(positions, freqs, length_dev, 1.0)
        with_cos = jnp.dot(stacked, cosine, precision=lax.Precision.HIGH)
        with_sin = jnp.dot(stacked, sine, precision=lax.Precision.HIGH)
        real_blocks.append(with_cos[:half] + with_sin[half:])
        imag_blocks.append(with_cos[half:] - with_sin[:half])
    return (jnp.concatenate(real_blocks, 1), jnp.concatenate(imag_blocks, 1))


def reorder_positions(arrived):
    channels, row_count, _, block_len = arrived.shape
    return jnp.swapaxes(arrived.reshape(channels, row_count, block_len), 1, 2).reshape(
        channels, row_count * block_len
    )


def local(tokens, norm_gain, w_in, w_out):
    length_dev = tokens.shape[0]
    row_count = lax.axis_size("row")
    col_count = lax.axis_size("col")
    total_len = length_dev * row_count
    widened = tokens.astype(jnp.float32)
    inverse = lax.rsqrt(jnp.mean(widened * widened, axis=1, keepdims=True) + NORM_EPS)
    normed = (widened * inverse * norm_gain[None, :]).astype(jnp.bfloat16)
    projected = lax.dot_general(
        w_in, normed, (((0,), (1,)), ((), ())), preferred_element_type=jnp.float32
    ).astype(jnp.bfloat16)
    channels = projected.shape[0]
    block_len = length_dev // row_count
    small_cos, small_sin = rotation_table(
        lax.broadcasted_iota(jnp.int32, (row_count, row_count), 0),
        lax.broadcasted_iota(jnp.int32, (row_count, row_count), 1),
        row_count,
        1.0 / math.sqrt(total_len),
    )
    per_row = channels // row_count
    arrived = lax.all_to_all(
        projected.reshape(channels, 1, length_dev), "row", split_axis=0, concat_axis=1, tiled=True
    )
    values = arrived.astype(jnp.float32)
    real_one = jnp.einsum("ka,cab->ckb", small_cos, values, precision=lax.Precision.HIGH)
    imag_one = -jnp.einsum("ka,cab->ckb", small_sin, values, precision=lax.Precision.HIGH)
    freq_index = lax.broadcasted_iota(jnp.int32, (row_count, length_dev), 0)
    pos_index = lax.broadcasted_iota(jnp.int32, (row_count, length_dev), 1)
    real_two, imag_two = twiddle(real_one, imag_one, freq_index, pos_index, total_len)
    stacked = jnp.concatenate(
        [
            real_two.reshape(per_row * row_count, length_dev),
            imag_two.reshape(per_row * row_count, length_dev),
        ],
        0,
    )
    real_three, imag_three = second_section(stacked, per_row * row_count)
    shaped = (per_row, row_count, row_count, block_len)
    back_real, back_imag = tuple(
        (
            part.astype(jnp.float32)
            for part in in_one_piece(
                (
                    real_three.reshape(shaped).astype(jnp.bfloat16),
                    imag_three.reshape(shaped).astype(jnp.bfloat16),
                ),
                "row",
                2,
                0,
                1,
            )
        )
    )
    spec_real = reorder_positions(back_real)
    spec_imag = reorder_positions(back_imag)
    quarter = length_dev // col_count
    group_cosine_table, group_sine_table = rotation_table(
        lax.broadcasted_iota(jnp.int32, (GROUP, GROUP), 0),
        lax.broadcasted_iota(jnp.int32, (GROUP, GROUP), 1),
        GROUP,
        1.0 / math.sqrt(GROUP),
    )
    real_input_values = lax.all_to_all(
        as_sent(spec_real.reshape(channels, col_count, quarter)),
        "col",
        split_axis=1,
        concat_axis=0,
        tiled=True,
    )
    imag_in = lax.all_to_all(
        as_sent(spec_imag.reshape(channels, col_count, quarter)),
        "col",
        split_axis=1,
        concat_axis=0,
        tiled=True,
    )
    width_all = real_input_values.shape[0]
    item_count = real_input_values.shape[2]
    groups = width_all // GROUP
    real_by_group = real_input_values.reshape(groups, GROUP, item_count)
    imaginary_by_group = imag_in.reshape(groups, GROUP, item_count)
    merged_spectrum = jnp.einsum(
        "hz,azo->aho", group_cosine_table, real_by_group, precision=lax.Precision.HIGH
    )
    merged_spectrum = merged_spectrum + jnp.einsum(
        "hz,azo->aho", group_sine_table, imaginary_by_group, precision=lax.Precision.HIGH
    )
    result = merged_spectrum.reshape(width_all, 1, item_count).astype(jnp.bfloat16)
    portion = lax.all_gather(result, "col", axis=2, tiled=True)
    flat = portion.reshape(portion.shape[0], portion.shape[2])
    output = lax.dot_general(
        flat, w_out, (((0,), (0,)), ((), ())), preferred_element_type=jnp.float32
    )
    return output.astype(jnp.bfloat16)


def solution(mesh):
    placed = (P("row", None), P(), P(None, "col"), P(None, "col"))
    return jax.shard_map(
        local, mesh=mesh, in_specs=placed, out_specs=P("row", "col"), check_vma=False
    )
```

profile of v0, /device:TPU:1, one launch (start us, length us, event | category | flops | bytes accessed | tf_op | source)
XLA Modules:
  0.0 170.5 jit_solution(13047247857492114618)
XLA Ops:
  6.5 3.2 %fusion = f32[1024]{0:T(1024)S(1)} fusion(bf16[1024,2048]{1,0:T(8,128)(2,1)} %param.4), kind=kLoop, calls=%fused_computation.2 | loop fusion | flops 6290432 | bytes 4198400 | tf_op jit(solution)/shard_map/reduce_sum | solution.py:78
  10.0 2.4 %fusion.38 = bf16[64,1,1024]{2,0,1:T(8,128)(2,1)S(1)} fusion(bf16[2048,64]{0,1:T(8,128)(2,1)} %param.6, bf16[1024,2048]{1,0:T(8,128)(2,1)S(1)} %copy-done.1, f32[2048]{0:T(1024)S(1)} %copy-done.2, f32[1024]{0:T(1024)S(1)} %add_rsqrt_fusion), kind=kOutput, calls=%fused_computation.44 | convolution fusion | flops 276889600 | bytes 4599808 | tf_op jit(solution)/shard_map/dot_general | solution.py:80
  13.0 0.7 reduce.1
  13.6 0.7 reshape.90
  14.3 13.9 %all-to-all-start = ((bf16[32,2,1024]{2,1,0:T(2,128)(2,1)}), bf16[32,2,1024]{2,1,0:T(2,128)(2,1)S(1)}, u32[]{:S(2)}, u32[]{:S(2)}) async-start(bf16[32,2,1024]{2,1,0:T(2,128)(2,1)} %reshape.90), calls=%async_computation | async-start | bytes 262144 | tf_op jit(solution)/shard_map/all_to_all | solution.py:92
  28.8 8.6 %all-to-all-done = bf16[32,2,1024]{2,1,0:T(2,128)(2,1)S(1)} async-done(((bf16[32,2,1024]{2,1,0:T(2,128)(2,1)}), bf16[32,2,1024]{2,1,0:T(2,128)(2,1)S(1)}, u32[]{:S(2)}, u32[]{:S(2)}) %all-to-all-start) | async-done | bytes 131104 | tf_op jit(solution)/shard_map/all_to_all | solution.py:92
  37.5 0.7 reduce
  38.9 8.7 %fusion.21 = f32[128,512]{1,0:T(8,128)S(1)} fusion(f32[64,1024]{1,0:T(8,128)S(1)} %bitcast.98, f32[64,1024]{1,0:T(8,128)S(1)} %bitcast.94), kind=kOutput, calls=%fused_computation.28 | convolution fusion | flops 410124288 | bytes 786432 | tf_op jit(solution)/shard_map/dot_general | solution.py:59
  47.6 8.6 %fusion.17 = f32[128,512]{1,0:T(8,128)S(1)} fusion(s32[512]{0:T(512)S(1)} %iota_add_fusion, f32[64,1024]{1,0:T(8,128)S(1)} %bitcast.99, f32[64,1024]{1,0:T(8,128)S(1)} %bitcast.95), kind=kOutput, calls=%fused_computation.24 | convolution fusion | flops 410124288 | bytes 788480 | tf_op jit(solution)/shard_map/dot_general | solution.py:58
  56.2 8.9 %fusion.15 = f32[128,512]{1,0:T(8,128)S(1)} fusion(s32[512]{0:T(512)S(1)} %iota_add_fusion, f32[64,1024]{1,0:T(8,128)S(1)} %bitcast.100, f32[64,1024]{1,0:T(8,128)S(1)} %bitcast.96), kind=kOutput, calls=%fused_computation.22 | convolution fusion | flops 410124288 | bytes 788480 | tf_op jit(solution)/shard_map/dot_general | solution.py:59
  65.1 8.6 %fusion.23 = f32[128,512]{1,0:T(8,128)S(1)} fusion(f32[64,1024]{1,0:T(8,128)S(1)} %bitcast.101, f32[64,1024]{1,0:T(8,128)S(1)} %bitcast.97), kind=kOutput, calls=%fused_computation.30 | convolution fusion | flops 410124288 | bytes 786432 | tf_op jit(solution)/shard_map/dot_general | solution.py:58
  74.2 0.7 copy.35
  76.6 13.7 %all_to_all.66 = bf16[32,2,2048]{2,1,0:T(2,128)(2,1)S(1)} all-to-all(bf16[32,2,2048]{2,1,0:T(2,128)(2,1)S(1)} %reshape.92), channel_id=1, replica_groups=mesh['row'=32,'col'=16] {'row'}, dimensions={0} | all-to-all | bytes 524288 | tf_op jit(solution)/shard_map/all_to_all | solution.py:19
  91.5 0.9 reshape.96
  92.4 10.9 %all-to-all-start.3 = ((bf16[16,2,2048]{2,1,0:T(2,128)(2,1)}), bf16[16,2,2048]{2,1,0:T(2,128)(2,1)S(1)}, u32[]{:S(2)}, u32[]{:S(2)}) async-start(bf16[16,2,2048]{2,1,0:T(2,128)(2,1)} %reshape.96), calls=%async_computation.3 | async-start | bytes 262144 | tf_op jit(solution)/shard_map/all_to_all | solution.py:141
  103.9 0.9 reshape.94
  104.8 7.4 %all-to-all-done.3 = bf16[16,2,2048]{2,1,0:T(2,128)(2,1)S(1)} async-done(((bf16[16,2,2048]{2,1,0:T(2,128)(2,1)}), bf16[16,2,2048]{2,1,0:T(2,128)(2,1)S(1)}, u32[]{:S(2)}, u32[]{:S(2)}) %all-to-all-start.3) | async-done | bytes 131104 | tf_op jit(solution)/shard_map/all_to_all | solution.py:141
  112.2 3.4 %all-to-all-start.2 = ((bf16[16,2,2048]{2,1,0:T(2,128)(2,1)}), bf16[16,2,2048]{2,1,0:T(2,128)(2,1)S(1)}, u32[]{:S(2)}, u32[]{:S(2)}) async-start(bf16[16,2,2048]{2,1,0:T(2,128)(2,1)} %reshape.94), calls=%async_computation.2 | async-start | bytes 262144 | tf_op jit(solution)/shard_map/all_to_all | solution.py:134
  116.3 8.2 %all-to-all-done.2 = bf16[16,2,2048]{2,1,0:T(2,128)(2,1)S(1)} async-done(((bf16[16,2,2048]{2,1,0:T(2,128)(2,1)}), bf16[16,2,2048]{2,1,0:T(2,128)(2,1)S(1)}, u32[]{:S(2)}, u32[]{:S(2)}) %all-to-all-start.2) | async-done | bytes 131104 | tf_op jit(solution)/shard_map/all_to_all | solution.py:134
  125.2 1.2 fusion.49
  126.4 1.2 fusion.37
  127.7 0.7 convert_element_type.118
  128.5 32.2 %all-gather.2.cloned.1.call-done = bf16[1024,1,1024]{0,2,1:T(8,128)(2,1)} async-done(((bf16[1024,1,64]{0,2,1:T(8,128)(2,1)}), bf16[1024,1,1024]{0,2,1:T(8,128)(2,1)}) %all-gather.2.cloned.1.call-update) | async-done | bytes 2097168 | tf_op jit(solution)/shard_map/all_gather | solution.py:160
  160.7 3.0 %fusion.29 = bf16[1024,128]{1,0:T(8,128)(2,1)} fusion(bf16[1024,128]{1,0:T(8,128)(2,1)S(1)} %copy-done, bf16[1024,1,1024]{0,2,1:T(8,128)(2,1)} %all-gather.2.cloned.1.call-done), kind=kOutput, calls=%fused_computation.36 | convolution fusion | flops 268566528 | bytes 2621440 | tf_op jit(solution)/shard_map/dot_general | solution.py:162
  (40 shorter events, 7.4 us)
Async XLA Ops:
  6.5 154.2 %copy-start = (bf16[1024,128]{1,0:T(8,128)(2,1)S(1)}, bf16[1024,128]{1,0:T(8,128)(2,1)}, u32[]{:S(2)}) copy-start(bf16[1024,128]{1,0:T(8,128)(2,1)} %param.7) | copy-start | bytes 786436
  6.5 3.5 %copy-start.1 = (bf16[1024,2048]{1,0:T(8,128)(2,1)S(1)}, bf16[1024,2048]{1,0:T(8,128)(2,1)}, u32[]{:S(2)}) copy-start(bf16[1024,2048]{1,0:T(8,128)(2,1)} %param.4) | copy-start | bytes 12582916
  6.5 3.5 %copy-start.2 = (f32[2048]{0:T(1024)S(1)}, f32[2048]{0:T(1024)}, u32[]{:S(2)}) copy-start(f32[2048]{0:T(1024)} %param.5) | copy-start | bytes 24580
  14.3 23.1 %all-to-all-start = ((bf16[32,2,1024]{2,1,0:T(2,128)(2,1)}), bf16[32,2,1024]{2,1,0:T(2,128)(2,1)S(1)}, u32[]{:S(2)}, u32[]{:S(2)}) async-start(bf16[32,2,1024]{2,1,0:T(2,128)(2,1)} %reshape.90), calls=%async_computation | async-start | bytes 262144 | tf_op jit(solution)/shard_map/all_to_all | solution.py:92
  92.4 19.8 %all-to-all-start.3 = ((bf16[16,2,2048]{2,1,0:T(2,128)(2,1)}), bf16[16,2,2048]{2,1,0:T(2,128)(2,1)S(1)}, u32[]{:S(2)}, u32[]{:S(2)}) async-start(bf16[16,2,2048]{2,1,0:T(2,128)(2,1)} %reshape.96), calls=%async_computation.3 | async-start | bytes 262144 | tf_op jit(solution)/shard_map/all_to_all | solution.py:141
  112.2 12.3 %all-to-all-start.2 = ((bf16[16,2,2048]{2,1,0:T(2,128)(2,1)}), bf16[16,2,2048]{2,1,0:T(2,128)(2,1)S(1)}, u32[]{:S(2)}, u32[]{:S(2)}) async-start(bf16[16,2,2048]{2,1,0:T(2,128)(2,1)} %reshape.94), calls=%async_computation.2 | async-start | bytes 262144 | tf_op jit(solution)/shard_map/all_to_all | solution.py:134
  115.6 45.1 %all-gather.2.cloned.1.call-start = ((), (), s32[]{:S(2)}) async-start(), calls=%async_computation.4 | async-start | bytes 2228224 | tf_op jit(solution)/shard_map/all_gather | solution.py:160
Sparse Core Ops, SparseCore 0:
  128.6 32.0 all-gather.1
where the time goes:
time: 171 us
  waiting for transfers between devices  56.5 us (33%)
  matrix products  43.2 us (25%)
  starting transfers between devices  28.2 us (16%)
  blocking collectives  13.7 us (8%)
  between operations  13.7 us (8%)
  local copies, waits for them, and re-layouts  9.71 us (6%)
  other arithmetic  5.56 us (3%)
    all_gather x1, waiting for transfers between devices, local(): portion = lax.all_gather(result, 'col', axis=2, tiled=True)  32.2 us
    dot_general x2, matrix products, second_section(): with_sin = jnp.dot(stacked, sine, precision=lax.Precision.HIGH)  17.6 us
    dot_general x2, matrix products, second_section(): with_cos = jnp.dot(stacked, cosine, precision=lax.Precision.HIGH)  17.2 us
    all_to_all x1, starting transfers between devices, local(): lax.all_to_all(projected.reshape(channels, 1, length_dev), 'row', split_a...  13.9 us
    all_to_all x1, blocking collectives, in_one_piece(): lax.all_to_all(both, axis, split_axis=split_dim, concat_axis=concat_dim,...  13.7 us
    all_to_all x1, starting transfers between devices, local(): lax.all_to_all(as_sent(spec_imag.reshape(channels, col_count, quarter)),...  10.9 us
    all_to_all x1, waiting for transfers between devices, local(): lax.all_to_all(projected.reshape(channels, 1, length_dev), 'row', split_a...  8.62 us
    all_to_all x1, waiting for transfers between devices, local(): lax.all_to_all(as_sent(spec_real.reshape(channels, col_count, quarter)),...  8.24 us
  transfers between devices with their start and end apart: 4, of which 4 were waited for; matrix products, arithmetic and copies ran while one was open for 2% of the time, Pallas kernels for 0%

commit v1 on v0

--- a/solution.py
+++ b/solution.py
@@ -157,7 +157,9 @@
         "hz,azo->aho", group_sine_table, imaginary_by_group, precision=lax.Precision.HIGH
     )
     result = merged_spectrum.reshape(width_all, 1, item_count).astype(jnp.bfloat16)
-    portion = lax.all_gather(result, "col", axis=2, tiled=True)
+    portion = jnp.concatenate(
+        lax.all_to_all(jnp.stack([result] * lax.axis_size("col")), "col", 0, 0), axis=2
+    )
     flat = portion.reshape(portion.shape[0], portion.shape[2])
     output = lax.dot_general(
         flat, w_out, (((0,), (0,)), ((), ())), preferred_element_type=jnp.float32

time: 171 us -> 176 us (1.029)
  blocking collectives: 13.7 us -> 67 us
  waiting for transfers between devices: 56.5 us -> 24.3 us
  between operations: 13.7 us -> 0.29 us
    all_to_all x0 -> x1, blocking collectives: none -> 53.3 us  [local(): lax.all_to_all(jnp.stack([result] * lax.axis_size('col')), 'col', 0, 0)]
    all_gather x1 -> x0, waiting for transfers between devices: 32.2 us -> none  [local(): portion = lax.all_gather(result, 'col', axis=2, tiled=True)]
  transfers between devices with their start and end apart: 4 -> 3, of which waited for: 4 -> 3; matrix products, arithmetic and copies ran while one was open for 2% -> 2% of each run, Pallas kernels for 0% -> 0%
where the time goes in v1:
time: 176 us
  blocking collectives  67 us (38%)
  matrix products  41.6 us (24%)
  starting transfers between devices  28.2 us (16%)
  waiting for transfers between devices  24.3 us (14%)
  local copies, waits for them, and re-layouts  9.13 us (5%)
  other arithmetic  5.56 us (3%)
    all_to_all x1, blocking collectives, local(): lax.all_to_all(jnp.stack([result] * lax.axis_size('col')), 'col', 0, 0)  53.3 us
    dot_general x2, matrix products, second_section(): with_sin = jnp.dot(stacked, sine, precision=lax.Precision.HIGH)  17.6 us
    dot_general x2, matrix products, second_section(): with_cos = jnp.dot(stacked, cosine, precision=lax.Precision.HIGH)  17.2 us
    all_to_all x1, starting transfers between devices, local(): lax.all_to_all(projected.reshape(channels, 1, length_dev), 'row', split_a...  13.9 us
    all_to_all x1, blocking collectives, in_one_piece(): lax.all_to_all(both, axis, split_axis=split_dim, concat_axis=concat_dim,...  13.7 us
    all_to_all x1, starting transfers between devices, local(): lax.all_to_all(as_sent(spec_imag.reshape(channels, col_count, quarter)),...  10.9 us
    all_to_all x1, waiting for transfers between devices, local(): lax.all_to_all(projected.reshape(channels, 1, length_dev), 'row', split_a...  8.62 us
    all_to_all x1, waiting for transfers between devices, local(): lax.all_to_all(as_sent(spec_real.reshape(channels, col_count, quarter)),...  8.29 us
  transfers between devices with their start and end apart: 3, of which 3 were waited for; matrix products, arithmetic and copies ran while one was open for 2% of the time, Pallas kernels for 0%

profile of v1, /device:TPU:1, one launch (start us, length us, event | category | flops | bytes accessed | tf_op | source)
XLA Modules:
  0.0 176.0 jit_solution(3199771472500739213)
XLA Ops:
  0.0 3.2 %fusion = f32[1024]{0:T(1024)S(1)} fusion(bf16[1024,2048]{1,0:T(8,128)(2,1)} %param.4), kind=kLoop, calls=%fused_computation.2 | loop fusion | flops 6290432 | bytes 4198400 | tf_op jit(solution)/shard_map/reduce_sum | solution.py:78
  3.5 2.4 %fusion.33 = bf16[64,1,1024]{2,0,1:T(8,128)(2,1)S(1)} fusion(bf16[2048,64]{0,1:T(8,128)(2,1)} %param.6, bf16[1024,2048]{1,0:T(8,128)(2,1)S(1)} %copy-done.1, f32[2048]{0:T(1024)S(1)} %copy-done.2, f32[1024]{0:T(1024)S(1)} %add_rsqrt_fusion), kind=kOutput, calls=%fused_computation.42 | convolution fusion | flops 276889600 | bytes 4599808 | tf_op jit(solution)/shard_map/dot_general | solution.py:80
  6.4 0.7 reduce.1
  7.1 0.7 reshape.89
  7.8 13.9 %all-to-all-start = ((bf16[32,2,1024]{2,1,0:T(2,128)(2,1)}), bf16[32,2,1024]{2,1,0:T(2,128)(2,1)S(1)}, u32[]{:S(2)}, u32[]{:S(2)}) async-start(bf16[32,2,1024]{2,1,0:T(2,128)(2,1)} %reshape.89), calls=%async_computation | async-start | bytes 262144 | tf_op jit(solution)/shard_map/all_to_all | solution.py:92
  22.2 8.6 %all-to-all-done = bf16[32,2,1024]{2,1,0:T(2,128)(2,1)S(1)} async-done(((bf16[32,2,1024]{2,1,0:T(2,128)(2,1)}), bf16[32,2,1024]{2,1,0:T(2,128)(2,1)S(1)}, u32[]{:S(2)}, u32[]{:S(2)}) %all-to-all-start) | async-done | bytes 131104 | tf_op jit(solution)/shard_map/all_to_all | solution.py:92
  31.0 0.7 reduce
  32.4 8.7 %fusion.19 = f32[128,512]{1,0:T(8,128)S(1)} fusion(f32[64,1024]{1,0:T(8,128)S(1)} %bitcast.100, f32[64,1024]{1,0:T(8,128)S(1)} %bitcast.96), kind=kOutput, calls=%fused_computation.26 | convolution fusion | flops 410124288 | bytes 786432 | tf_op jit(solution)/shard_map/dot_general | solution.py:59
  41.1 8.6 %fusion.15 = f32[128,512]{1,0:T(8,128)S(1)} fusion(s32[512]{0:T(512)S(1)} %iota_add_fusion, f32[64,1024]{1,0:T(8,128)S(1)} %bitcast.101, f32[64,1024]{1,0:T(8,128)S(1)} %bitcast.97), kind=kOutput, calls=%fused_computation.22 | convolution fusion | flops 410124288 | bytes 788480 | tf_op jit(solution)/shard_map/dot_general | solution.py:58
  49.7 8.9 %fusion.13 = f32[128,512]{1,0:T(8,128)S(1)} fusion(s32[512]{0:T(512)S(1)} %iota_add_fusion, f32[64,1024]{1,0:T(8,128)S(1)} %bitcast.102, f32[64,1024]{1,0:T(8,128)S(1)} %bitcast.98), kind=kOutput, calls=%fused_computation.20 | convolution fusion | flops 410124288 | bytes 788480 | tf_op jit(solution)/shard_map/dot_general | solution.py:59
  58.6 8.6 %fusion.21 = f32[128,512]{1,0:T(8,128)S(1)} fusion(f32[64,1024]{1,0:T(8,128)S(1)} %bitcast.103, f32[64,1024]{1,0:T(8,128)S(1)} %bitcast.99), kind=kOutput, calls=%fused_computation.28 | convolution fusion | flops 410124288 | bytes 786432 | tf_op jit(solution)/shard_map/dot_general | solution.py:58
  67.7 0.7 copy.34
  68.7 0.7 copy.33
  70.1 13.7 %all_to_all.71 = bf16[32,2,2048]{2,1,0:T(2,128)(2,1)S(1)} all-to-all(bf16[32,2,2048]{2,1,0:T(2,128)(2,1)S(1)} %reshape.91), channel_id=1, replica_groups=mesh['row'=32,'col'=16] {'row'}, dimensions={0} | all-to-all | bytes 524288 | tf_op jit(solution)/shard_map/all_to_all | solution.py:19
  85.0 0.9 reshape.95
  85.9 10.9 %all-to-all-start.3 = ((bf16[16,2,2048]{2,1,0:T(2,128)(2,1)}), bf16[16,2,2048]{2,1,0:T(2,128)(2,1)S(1)}, u32[]{:S(2)}, u32[]{:S(2)}) async-start(bf16[16,2,2048]{2,1,0:T(2,128)(2,1)} %reshape.95), calls=%async_computation.3 | async-start | bytes 262144 | tf_op jit(solution)/shard_map/all_to_all | solution.py:141
  97.4 0.9 reshape.93
  98.3 7.4 %all-to-all-done.3 = bf16[16,2,2048]{2,1,0:T(2,128)(2,1)S(1)} async-done(((bf16[16,2,2048]{2,1,0:T(2,128)(2,1)}), bf16[16,2,2048]{2,1,0:T(2,128)(2,1)S(1)}, u32[]{:S(2)}, u32[]{:S(2)}) %all-to-all-start.3) | async-done | bytes 131104 | tf_op jit(solution)/shard_map/all_to_all | solution.py:141
  105.6 3.4 %all-to-all-start.2 = ((bf16[16,2,2048]{2,1,0:T(2,128)(2,1)}), bf16[16,2,2048]{2,1,0:T(2,128)(2,1)S(1)}, u32[]{:S(2)}, u32[]{:S(2)}) async-start(bf16[16,2,2048]{2,1,0:T(2,128)(2,1)} %reshape.93), calls=%async_computation.2 | async-start | bytes 262144 | tf_op jit(solution)/shard_map/all_to_all | solution.py:134
  109.7 8.3 %all-to-all-done.2 = bf16[16,2,2048]{2,1,0:T(2,128)(2,1)S(1)} async-done(((bf16[16,2,2048]{2,1,0:T(2,128)(2,1)}), bf16[16,2,2048]{2,1,0:T(2,128)(2,1)S(1)}, u32[]{:S(2)}, u32[]{:S(2)}) %all-to-all-start.2) | async-done | bytes 131104 | tf_op jit(solution)/shard_map/all_to_all | solution.py:134
  118.6 1.2 fusion.44
  119.8 1.2 fusion.32
  121.3 53.3 %all_to_all.72 = bf16[16,1024,1,64]{1,3,2,0:T(8,128)(2,1)S(1)} all-to-all(bf16[16,1024,1,64]{1,3,2,0:T(8,128)(2,1)S(1)} %stack.2), channel_id=1, replica_groups=mesh['row'=32,'col'=16] {'col'}, dimensions={0} | all-to-all | bytes 4194304 | tf_op jit(solution)/shard_map/all_to_all | solution.py:161
  174.6 1.4 convolution_convert_fusion
  (38 shorter events, 6.8 us)
Async XLA Ops:
  0.0 174.6 %copy-start = (bf16[1024,128]{1,0:T(8,128)(2,1)S(1)}, bf16[1024,128]{1,0:T(8,128)(2,1)}, u32[]{:S(2)}) copy-start(bf16[1024,128]{1,0:T(8,128)(2,1)} %param.7) | copy-start | bytes 786436
  0.0 3.5 %copy-start.1 = (bf16[1024,2048]{1,0:T(8,128)(2,1)S(1)}, bf16[1024,2048]{1,0:T(8,128)(2,1)}, u32[]{:S(2)}) copy-start(bf16[1024,2048]{1,0:T(8,128)(2,1)} %param.4) | copy-start | bytes 12582916
  0.0 3.5 %copy-start.2 = (f32[2048]{0:T(1024)S(1)}, f32[2048]{0:T(1024)}, u32[]{:S(2)}) copy-start(f32[2048]{0:T(1024)} %param.5) | copy-start | bytes 24580
  7.8 23.1 %all-to-all-start = ((bf16[32,2,1024]{2,1,0:T(2,128)(2,1)}), bf16[32,2,1024]{2,1,0:T(2,128)(2,1)S(1)}, u32[]{:S(2)}, u32[]{:S(2)}) async-start(bf16[32,2,1024]{2,1,0:T(2,128)(2,1)} %reshape.89), calls=%async_computation | async-start | bytes 262144 | tf_op jit(solution)/shard_map/all_to_all | solution.py:92
  85.9 19.8 %all-to-all-start.3 = ((bf16[16,2,2048]{2,1,0:T(2,128)(2,1)}), bf16[16,2,2048]{2,1,0:T(2,128)(2,1)S(1)}, u32[]{:S(2)}, u32[]{:S(2)}) async-start(bf16[16,2,2048]{2,1,0:T(2,128)(2,1)} %reshape.95), calls=%async_computation.3 | async-start | bytes 262144 | tf_op jit(solution)/shard_map/all_to_all | solution.py:141
  105.6 12.3 %all-to-all-start.2 = ((bf16[16,2,2048]{2,1,0:T(2,128)(2,1)}), bf16[16,2,2048]{2,1,0:T(2,128)(2,1)S(1)}, u32[]{:S(2)}, u32[]{:S(2)}) async-start(bf16[16,2,2048]{2,1,0:T(2,128)(2,1)} %reshape.93), calls=%async_computation.2 | async-start | bytes 262144 | tf_op jit(solution)/shard_map/all_to_all | solution.py:134
